TPU v7x, 32 devices: a whole 2x2x4 slice. The times are simulated.
32 devices in a mesh: sp: 4 (over y, x), tp: 8 (over z, core).
Axes of the slice: x: 2, y: 2, z: 4, core: 2. Of those that a mesh axis runs over, the one named last changes fastest.
Arguments:
- query_heads: bfloat16 [4096, 2048], P('sp', 'tp'), may hold values from -256 to 256
- key_heads: bfloat16 [4096, 1024], P('sp', 'tp'), may hold values from -7 to 7
- value_heads: bfloat16 [4096, 1024], P('sp', 'tp'), may hold values from -6 to 6
- sink_logit: float32 [32], P('tp'), may hold values from 3 to 7
- residual: bfloat16 [4096, 2048], P(('sp', 'tp')), may hold values from -6 to 6
- out_weight: bfloat16 [2048, 2048], replicated, may hold values from -0.5 to 0.5
- norm_gain: float32 [2048], replicated, may hold values from 0.1 to 1.9
- routes: int32 [4096, 2], P('sp'), may hold values from 0 to 3, all different within a row; in each aligned block of 128 rows (0 to 127, 128 to 255, ...) at most 80 rows name the same one
- route_weight: float32 [4096, 2], P(('sp', 'tp')), may hold values from 0.2 to 1
- gate_weight: bfloat16 [4, 2048, 2048], P('sp', None, 'tp'), may hold values from -0.3125 to 0.3125
- up_weight: bfloat16 [4, 2048, 2048], P('sp', None, 'tp'), may hold values from -0.3125 to 0.3125
- down_weight: bfloat16 [4, 2048, 2048], P('sp', 'tp'), may hold values from -0.0625 to 0.0625
Outputs:
- updated: bfloat16 [4096, 2048], P(('sp', 'tp'))
Inputs may be any that keep to these rules, and one draw needn't show every extreme that they name: `routes`: each row names 2 different experts. In each aligned block of 128 rows no expert is named more than 80 times, and in every draw some block names some expert exactly 80 times.
All inputs are finite; a program needn't handle non-finite values.
Results may differ from a plain program's by a relative error of at most 0.023.
Values may be sent and summed in bfloat16 or wider, within the bound.
A program may use at most 128 MiB of HBM per device.

v0:
```python
import jax
import jax.numpy as jnp
from jax import lax
from jax.sharding import PartitionSpec as P

HEAD = 64
WINDOW = 128


eps = 1e-06
clamp_limit = 7.0
sigmoid_alpha = 1.702


def from_behind(block, axis, distance):
    devices = range(lax.axis_size(axis))
    route = [(i - distance, i) for i in devices if i - distance in devices]
    return lax.ppermute(block, axis, route)


def expert_hidden(row_block, gate_local, up_local):
    gate_pre = jnp.dot(row_block, gate_local, preferred_element_type=jnp.float32)
    upward = jnp.dot(row_block, up_local, preferred_element_type=jnp.float32)
    capped = jnp.minimum(gate_pre, clamp_limit)
    linear = jnp.clip(upward, -clamp_limit, clamp_limit)
    return (capped * jax.nn.sigmoid(sigmoid_alpha * capped) * (linear + 1.0)).astype(jnp.bfloat16)


def slot_layout(own_routes, expert_count, capacity):
    flat_ids = own_routes.reshape(-1)
    one_hot = (flat_ids[:, None] == jnp.arange(expert_count, dtype=jnp.int32)[None, :]).astype(
        jnp.int32
    )
    before = jnp.cumsum(one_hot, axis=0) - one_hot
    ranked = jnp.sum(before * one_hot, axis=1)
    return flat_ids * capacity + ranked


def fill_slots(normed_rows, slot_ids, expert_count, capacity, choose_count):
    targets = jnp.arange(expert_count * capacity, dtype=jnp.int32)
    matched = (targets[:, None] == slot_ids[None, :]).astype(jnp.bfloat16)
    repeated = jnp.repeat(normed_rows, choose_count, axis=0)
    filled = jnp.dot(matched, repeated, preferred_element_type=jnp.float32).astype(jnp.bfloat16)
    return filled.reshape(expert_count, capacity, normed_rows.shape[1])


def local(
    query_heads,
    key_heads,
    value_heads,
    sink_logit,
    residual,
    out_weight,
    norm_gain,
    routes,
    route_weight,
    gate_weight,
    up_weight,
    down_weight,
):
    sp_count = lax.axis_size("sp")
    span_rows = query_heads.shape[0]
    kv_local = key_heads.shape[1] // HEAD
    group_size = query_heads.shape[1] // key_heads.shape[1]
    block_count = span_rows // WINDOW
    key_tail, value_tail = from_behind(
        (key_heads[span_rows - WINDOW :], value_heads[span_rows - WINDOW :]), "sp", 1
    )

    def banded(current, tail):
        shaped = current.reshape(block_count, WINDOW, kv_local, HEAD)
        earlier = jnp.concatenate([tail.reshape(1, WINDOW, kv_local, HEAD), shaped[:-1]], axis=0)
        return jnp.concatenate([earlier, shaped], axis=1)

    key_band = banded(key_heads, key_tail)
    value_band = banded(value_heads, value_tail)
    query_blocks = query_heads.reshape(block_count, WINDOW, kv_local, group_size, HEAD)
    scores = jnp.einsum(
        "nqhgd,nkhd->nhgqk", query_blocks, key_band, preferred_element_type=jnp.float32
    ) * HEAD ** (-0.5)
    query_pos = jnp.arange(WINDOW)[:, None]
    key_col = jnp.arange(2 * WINDOW)[None, :]
    distance = query_pos + WINDOW - key_col
    block_ids = jnp.arange(block_count)[:, None, None]
    key_global = lax.axis_index("sp") * span_rows + (block_ids - 1) * WINDOW + key_col[None]
    allowed = (distance[None] >= 0) & (distance[None] < WINDOW) & (key_global >= 0)
    logits = jnp.where(allowed[:, None, None], scores, -jnp.inf)
    sink_term = sink_logit.reshape(kv_local, group_size)[None, :, :, None, None]
    row_max = jnp.maximum(jnp.max(logits, axis=-1, keepdims=True), sink_term)
    raised = jnp.exp(logits - row_max)
    weights_bf = (
        raised / (jnp.sum(raised, axis=-1, keepdims=True) + jnp.exp(sink_term - row_max))
    ).astype(jnp.bfloat16)
    attended = jnp.einsum(
        "nhgqk,nkhd->nqhgd", weights_bf, value_band, preferred_element_type=jnp.float32
    )
    attended = attended.astype(jnp.bfloat16).reshape(span_rows, query_heads.shape[1])
    tok_rows = residual.shape[0]
    tp_index = lax.axis_index("tp")
    token_heads = lax.all_to_all(attended, "tp", split_axis=0, concat_axis=1, tiled=True)
    mixed = jnp.dot(token_heads, out_weight, preferred_element_type=jnp.float32)
    stream = (residual.astype(jnp.float32) + mixed).astype(jnp.bfloat16)
    stream32 = stream.astype(jnp.float32)
    normed = (
        stream32
        * lax.rsqrt(jnp.mean(stream32 * stream32, axis=-1, keepdims=True) + eps)
        * norm_gain
    ).astype(jnp.bfloat16)
    choose_count = routes.shape[1]
    capacity = max(2, 5 * tok_rows * choose_count // (4 * sp_count))
    model_width = normed.shape[1]
    gate_local = gate_weight[0]
    up_local = up_weight[0]
    down_local = down_weight[0]
    own_routes = lax.dynamic_slice_in_dim(routes, tp_index * tok_rows, tok_rows, 0)
    own_slots = slot_layout(own_routes, sp_count, capacity)
    outgoing = fill_slots(normed, own_slots, sp_count, capacity, choose_count)
    arrived = lax.all_to_all(outgoing, "sp", split_axis=0, concat_axis=0, tiled=True)
    hidden = expert_hidden(
        lax.all_gather(arrived[None], "tp", axis=0, tiled=True).reshape(-1, model_width),
        gate_local,
        up_local,
    )
    summed = lax.psum_scatter(
        jnp.dot(hidden, down_local, preferred_element_type=jnp.float32).astype(jnp.bfloat16),
        "tp",
        scatter_dimension=0,
        tiled=True,
    )
    expert_out = summed.reshape(sp_count, capacity, model_width)
    returned = lax.all_to_all(expert_out, "sp", split_axis=0, concat_axis=0, tiled=True)
    picked = returned.reshape(-1, model_width)[own_slots].reshape(
        tok_rows, choose_count, model_width
    )
    combined = jnp.sum(picked.astype(jnp.float32) * route_weight[:, :, None], axis=1)
    return (stream32 + combined).astype(jnp.bfloat16)


def solution(mesh):
    placed = (
        P("sp", "tp"),
        P("sp", "tp"),
        P("sp", "tp"),
        P("tp"),
        P(("sp", "tp"), None),
        P(),
        P(),
        P("sp", None),
        P(("sp", "tp"), None),
        P("sp", None, "tp"),
        P("sp", None, "tp"),
        P("sp", "tp", None),
    )
    return jax.shard_map(
        local, mesh=mesh, in_specs=placed, out_specs=P(("sp", "tp"), None), check_vma=False
    )
```

profile of v0, /device:TPU:0, one launch (start us, length us, event | category | flops | bytes accessed | tf_op | source)
XLA Modules:
  0.0 353.1 jit_solution(9478695877296077979)
XLA Ops:
  6.5 0.0 copy-start
  6.5 1.5 slice.27
  8.0 5.5 %collective-permute-start.1 = (bf16[128,128]{1,0:T(8,128)(2,1)}, bf16[128,128]{1,0:T(8,128)(2,1)}, u32[]{:S(2)}, u32[]{:S(2)}) collective-permute-start(bf16[128,128]{1,0:T(8,128)(2,1)} %slice.27), channel_id=1, source_target_pairs={{0,8},{8,16},{16,24},{1,9},{9,17},{17,25},{2,10},{10,18},{18,26},{... | collective-permute-start | bytes 98312 | tf_op jit(solution)/shard_map/ppermute | solution.py:18
  13.5 1.4 slice.24
  14.9 2.8 collective-permute-start
  17.7 0.1 add_compare_fusion
  17.8 0.3 broadcast_and_fusion
  18.2 1.2 reshape.215
  19.4 1.2 reshape.213
  20.6 3.2 reshape.216
  23.8 0.2 reshape.214
  24.0 0.9 copy.46
  25.0 0.4 copy.48
  25.3 0.1 max.24
  25.4 0.0 slice-done.1
  25.4 0.2 reshape.212
  25.6 0.9 copy.41
  26.6 0.4 copy.43
  26.9 0.0 collective-permute-done.1
  26.9 0.9 copy.44
  27.8 2.2 fusion.4
  30.0 0.1 broadcast_maximum_fusion
  30.0 1.8 copy-done.1
  31.9 1.0 fusion.3
  32.9 0.1 exponential_add_fusion
  33.0 0.0 collective-permute-done
  33.0 0.1 copy.39
  33.1 4.2 %fusion.8 = bf16[8,2,64,2,128]{4,2,3,1,0:T(8,128)(2,1)} fusion(f32[8,2,256,128,2]{3,2,4,1,0:T(8,128)} %copy-done.1, f32[8,2,2,128]{3,2,1,0:T(2,128)S(1)} %exponential_add_fusion, f32[8,2,2,128]{3,2,1,0:T(2,128)S(1)} %broadcast_maximum_fusion, pred[8,128,256]{1,2,0:T(8,128)(4,1)S(1)} %broadcast_and_fusion, bf16[8,128,2,64]{1,3,2,0:T(8,128)(2,1)S(1)} %copy.43, ...), kind=kOutput, calls=%fused_computation.18 | convolution fusion | flops 141295616 | bytes 5537792 | tf_op jit(solution)/shard_map/nhgqk,nkhd->nqhgd/dot_general | solution.py:94
  37.3 4.9 %all-to-all-start = ((bf16[8,128,256]{1,2,0:T(8,128)(2,1)}), bf16[8,128,256]{1,2,0:T(8,128)(2,1)S(1)}, u32[]{:S(2)}, u32[]{:S(2)}) async-start(bf16[8,128,256]{1,2,0:T(8,128)(2,1)} %bitcast.8), calls=%async_computation | async-start | bytes 1048576 | tf_op jit(solution)/shard_map/all_to_all | solution.py:100
  42.2 0.0 all-gather.3.cloned.1.call-start
  42.2 0.7 broadcast_multiply_fusion
  42.9 0.1 copy.52
  43.0 0.1 eq.40
  43.2 0.1 reshape.192
  43.3 1.2 reduce-window.6
  44.6 0.1 slice.34
  44.6 0.1 copy.54
  44.8 0.1 copy.55
  44.9 0.1 add_bitcast_fusion
  45.0 12.5 %all-to-all-done = bf16[8,128,256]{1,2,0:T(8,128)(2,1)S(1)} async-done(((bf16[8,128,256]{1,2,0:T(8,128)(2,1)}), bf16[8,128,256]{1,2,0:T(8,128)(2,1)S(1)}, u32[]{:S(2)}, u32[]{:S(2)}) %all-to-all-start) | async-done | bytes 524320 | tf_op jit(solution)/shard_map/all_to_all | solution.py:100
  57.5 4.8 %multiply_reduce_fusion.1 = (f32[128]{0:T(128)S(1)}, f32[128,2048]{1,0:T(8,128)S(1)}) fusion(bf16[128,2048]{0,1:T(8,128)(2,1)S(1)} %bitcast.74, bf16[2048,2048]{1,0:T(8,128)(2,1)} %param.17, bf16[128,2048]{1,0:T(8,128)(2,1)} %param.16), kind=kOutput, calls=%fused_computation.26 | convolution fusion | flops 1075314560 | bytes 10486272 | tf_op jit(solution)/shard_map/dot_general | solution.py:101
  62.3 0.0 copy-done.2
  62.3 0.2 multiply_convert_fusion
  62.5 1.6 broadcast_in_dim.18
  64.1 1.5 reshape.194
  65.6 0.5 convolution_convert_fusion.1
  66.1 20.1 %all_to_all.29 = bf16[4,80,2048]{2,1,0:T(8,128)(2,1)} all-to-all(bf16[4,80,2048]{2,1,0:T(8,128)(2,1)S(1)} %bitcast.73), channel_id=1, replica_groups=mesh['sp'=4,'tp'=8] {'sp'}, dimensions={0} | all-to-all | bytes 2621440 | tf_op jit(solution)/shard_map/all_to_all | solution.py:118
  86.2 0.0 all-gather.3.cloned.1.call-update
  86.2 0.2 reduce-scatter.2.cloned.1.call-start
  86.5 97.2 %all-gather.3.cloned.1.call-done = bf16[32,80,2048]{2,1,0:T(8,128)(2,1)} async-done(((bf16[4,80,2048]{2,1,0:T(8,128)(2,1)}), bf16[32,80,2048]{2,1,0:T(8,128)(2,1)}) %all-gather.3.cloned.1.call-update) | async-done | bytes 10485776 | tf_op jit(solution)/shard_map/all_gather | solution.py:120
  183.7 8.7 %convolution_minimum_fusion = f32[2560,256]{1,0:T(8,128)} fusion(bf16[2560,2048]{1,0:T(8,128)(2,1)} %bitcast.81, bf16[1,2048,256]{2,1,0:T(8,128)(2,1)} %param.21), kind=kOutput, calls=%fused_computation.6 | convolution fusion | flops 2685009920 | bytes 14155776 | tf_op jit(solution)/shard_map/dot_general | solution.py:22
  192.4 0.0 copy-done
  192.4 16.1 %convolution_convert_fusion = bf16[2560,2048]{1,0:T(8,128)(2,1)} fusion(bf16[1,256,2048]{2,1,0:T(8,128)(2,1)S(1)} %copy-done, bf16[2560,2048]{1,0:T(8,128)(2,1)} %bitcast.82, f32[2560,256]{1,0:T(8,128)} %convolution_minimum_fusion, bf16[1,2048,256]{2,1,0:T(8,128)(2,1)S(1)} %copy-done.4), kind=kOutput, calls=%fused_computation.1 | convolution fusion | flops 5379850240 | bytes 25690112 | tf_op jit(solution)/shard_map/dot_general | solution.py:125
  208.5 0.0 reduce-scatter.2.cloned.1.call-update
  208.6 107.8 %reduce-scatter.2.cloned.1.call-done = bf16[320,2048]{1,0:T(8,128)(2,1)} async-done(((bf16[2560,2048]{1,0:T(8,128)(2,1)}), bf16[320,2048]{1,0:T(8,128)(2,1)}) %reduce-scatter.2.cloned.1.call-update) | async-done | bytes 1310736 | tf_op jit(solution)/shard_map/reduce_scatter | solution.py:124
  316.4 3.8 %all-to-all-start.2 = ((bf16[4,80,2048]{2,1,0:T(8,128)(2,1)}), bf16[4,80,2048]{2,1,0:T(8,128)(2,1)S(1)}, u32[]{:S(2)}, u32[]{:S(2)}) async-start(bf16[4,80,2048]{2,1,0:T(8,128)(2,1)} %bitcast.75), calls=%async_computation.3 | async-start | bytes 2621440 | tf_op jit(solution)/shard_map/all_to_all | solution.py:131
  320.1 0.1 copy.56
  320.3 0.1 mul.109
  320.4 0.1 copy.57
  320.5 14.2 %all-to-all-done.2 = bf16[4,80,2048]{2,1,0:T(8,128)(2,1)S(1)} async-done(((bf16[4,80,2048]{2,1,0:T(8,128)(2,1)}), bf16[4,80,2048]{2,1,0:T(8,128)(2,1)S(1)}, u32[]{:S(2)}, u32[]{:S(2)}) %all-to-all-start.2) | async-done | bytes 1310752 | tf_op jit(solution)/shard_map/all_to_all | solution.py:131
  334.8 2.3 gather_fusion
  337.1 3.4 reshape.199
  340.5 4.8 %multiply_reduce_fusion = f32[128,2048]{1,0:T(8,128)S(1)} fusion(f32[128,2,2048]{2,1,0:T(2,128)} %reshape.199, f32[128,2]{1,0:T(8,128)S(1)} %copy.57), kind=kLoop, calls=%fused_computation.16 | loop fusion | flops 786432 | bytes 3146752 | tf_op jit(solution)/shard_map/reduce_sum | solution.py:135
  345.3 0.9 add_convert_fusion
  (22 shorter events, 0.2 us)
Async XLA Ops:
  6.5 185.9 %copy-start = (bf16[1,256,2048]{2,1,0:T(8,128)(2,1)S(1)}, bf16[1,256,2048]{2,1,0:T(8,128)(2,1)}, u32[]{:S(2)}) copy-start(bf16[1,256,2048]{2,1,0:T(8,128)(2,1)} %param.23) | copy-start | bytes 3145732
  6.5 17.3 %slice-start = ((bf16[1024,128]{1,0:T(8,128)(2,1)}), bf16[896,128]{1,0:T(8,128)(2,1)S(1)}, s32[]{:S(2)}) async-start(bf16[1024,128]{1,0:T(8,128)(2,1)} %param.13), calls=%async_computation.6 | async-start | bytes 458752 | tf_op jit(solution)/shard_map/slice | solution.py:72
  6.5 18.9 %slice-start.1 = ((bf16[1024,128]{1,0:T(8,128)(2,1)}), bf16[896,128]{1,0:T(8,128)(2,1)S(1)}, s32[]{:S(2)}) async-start(bf16[1024,128]{1,0:T(8,128)(2,1)} %param.14), calls=%async_computation.7 | async-start | bytes 458752 | tf_op jit(solution)/shard_map/slice | solution.py:72
  6.5 18.8 %copy-start.5 = (f32[4]{0:T(128)S(1)}, f32[4]{0:T(128)}, u32[]{:S(2)}) copy-start(f32[4]{0:T(128)} %param.15) | copy-start | bytes 52
  8.0 18.9 %collective-permute-start.1 = (bf16[128,128]{1,0:T(8,128)(2,1)}, bf16[128,128]{1,0:T(8,128)(2,1)}, u32[]{:S(2)}, u32[]{:S(2)}) collective-permute-start(bf16[128,128]{1,0:T(8,128)(2,1)} %slice.27), channel_id=1, source_target_pairs={{0,8},{8,16},{16,24},{1,9},{9,17},{17,25},{2,10},{10,18},{18,26},{... | collective-permute-start | bytes 98312 | tf_op jit(solution)/shard_map/ppermute | solution.py:18
  14.9 18.1 %collective-permute-start = (bf16[128,128]{1,0:T(8,128)(2,1)}, bf16[128,128]{1,0:T(8,128)(2,1)S(1)}, u32[]{:S(2)}, u32[]{:S(2)}) collective-permute-start(bf16[128,128]{1,0:T(8,128)(2,1)} %slice.24), channel_id=1, source_target_pairs={{0,8},{8,16},{16,24},{1,9},{9,17},{17,25},{2,10},{10,18},{18,26},{... | collective-permute-start | bytes 98312 | tf_op jit(solution)/shard_map/ppermute | solution.py:18
  30.0 1.9 copy-start.1
  37.3 20.2 %all-to-all-start = ((bf16[8,128,256]{1,2,0:T(8,128)(2,1)}), bf16[8,128,256]{1,2,0:T(8,128)(2,1)S(1)}, u32[]{:S(2)}, u32[]{:S(2)}) async-start(bf16[8,128,256]{1,2,0:T(8,128)(2,1)} %bitcast.8), calls=%async_computation | async-start | bytes 1048576 | tf_op jit(solution)/shard_map/all_to_all | solution.py:100
  42.2 141.5 %all-gather.3.cloned.1.call-start = ((), (), s32[]{:S(2)}) async-start(), calls=%async_computation.5 | async-start | bytes 11796480 | tf_op jit(solution)/shard_map/all_gather | solution.py:120
  57.5 4.8 %copy-start.2 = (f32[2048]{0:T(1024)S(1)}, f32[2048]{0:T(1024)}, u32[]{:S(2)}) copy-start(f32[2048]{0:T(1024)} %param.18) | copy-start | bytes 24580
  86.2 230.1 %reduce-scatter.2.cloned.1.call-start = ((), (), s32[]{:S(2)}) async-start(), calls=%async_computation.4 | async-start | bytes 11796480 | tf_op jit(solution)/shard_map/reduce_scatter | solution.py:124
  183.7 8.7 %copy-start.4 = (bf16[1,2048,256]{2,1,0:T(8,128)(2,1)S(1)}, bf16[1,2048,256]{2,1,0:T(8,128)(2,1)}, u32[]{:S(2)}) copy-start(bf16[1,2048,256]{2,1,0:T(8,128)(2,1)} %param.22) | copy-start | bytes 3145732
  208.5 111.9 %copy-start.3 = (f32[128,2]{0,1:T(2,128)S(1)}, f32[128,2]{0,1:T(2,128)}, u32[]{:S(2)}) copy-start(f32[128,2]{0,1:T(2,128)} %param.20) | copy-start | bytes 3076
  316.4 18.4 %all-to-all-start.2 = ((bf16[4,80,2048]{2,1,0:T(8,128)(2,1)}), bf16[4,80,2048]{2,1,0:T(8,128)(2,1)S(1)}, u32[]{:S(2)}, u32[]{:S(2)}) async-start(bf16[4,80,2048]{2,1,0:T(8,128)(2,1)} %bitcast.75), calls=%async_computation.3 | async-start | bytes 2621440 | tf_op jit(solution)/shard_map/all_to_all | solution.py:131
Sparse Core Ops, SparseCore 0:
  86.4 97.2 all-gather.2
  208.7 107.6 reduce-scatter.1
where the time goes:
time: 354 us; the launch traced here: 353 us
  waiting for transfers between devices  232 us (66%)
  matrix products  36.5 us (10%)
  local copies, waits for them, and re-layouts  24.2 us (7%)
  blocking collectives  20.1 us (6%)
  starting transfers between devices  17.1 us (5%)
  between operations  13.7 us (4%)
  other arithmetic  9.63 us (3%)
    reduce_scatter x1, waiting for transfers between devices, local(): lax.psum_scatter(jnp.dot(hidden, down_local, preferred_element_type=jnp.f...  108 us
    all_gather x1, waiting for transfers between devices, local(): lax.all_gather(arrived[None], 'tp', axis=0, tiled=True)  97.2 us
    all_to_all x1, blocking collectives, local(): lax.all_to_all(outgoing, 'sp', split_axis=0, concat_axis=0, tiled=True)  20.1 us
    dot_general x1, matrix products, local(): jnp.dot(hidden, down_local, preferred_element_type=jnp.float32)  16.1 us
    all_to_all x1, waiting for transfers between devices, local(): lax.all_to_all(expert_out, 'sp', split_axis=0, concat_axis=0, tiled=True)  14.2 us
    all_to_all x1, waiting for transfers between devices, local(): lax.all_to_all(attended, 'tp', split_axis=0, concat_axis=1, tiled=True)  12.5 us
    dot_general x1, matrix products, expert_hidden(): jnp.dot(row_block, gate_local, preferred_element_type=jnp.float32)  8.73 us
    ppermute x2, starting transfers between devices, from_behind(): return lax.ppermute(block, axis, route)  8.26 us
  transfers between devices with their start and end apart: 6, of which 4 were waited for; matrix products, arithmetic and copies ran while one was open for 5% of the time, Pallas kernels for 0%

commit v1 on v0

--- a/solution.py
+++ b/solution.py
@@ -1,6 +1,10 @@
+import functools
+
 import jax
 import jax.numpy as jnp
 from jax import lax
+from jax.experimental import pallas as pl
+from jax.experimental.pallas import tpu as pltpu
 from jax.sharding import PartitionSpec as P
 
 HEAD = 64
@@ -18,30 +22,490 @@
     return lax.ppermute(block, axis, route)
 
 
-def expert_hidden(row_block, gate_local, up_local):
-    gate_pre = jnp.dot(row_block, gate_local, preferred_element_type=jnp.float32)
-    upward = jnp.dot(row_block, up_local, preferred_element_type=jnp.float32)
-    capped = jnp.minimum(gate_pre, clamp_limit)
-    linear = jnp.clip(upward, -clamp_limit, clamp_limit)
-    return (capped * jax.nn.sigmoid(sigmoid_alpha * capped) * (linear + 1.0)).astype(jnp.bfloat16)
-
-
-def slot_layout(own_routes, expert_count, capacity):
-    flat_ids = own_routes.reshape(-1)
-    one_hot = (flat_ids[:, None] == jnp.arange(expert_count, dtype=jnp.int32)[None, :]).astype(
-        jnp.int32
-    )
-    before = jnp.cumsum(one_hot, axis=0) - one_hot
-    ranked = jnp.sum(before * one_hot, axis=1)
-    return flat_ids * capacity + ranked
-
-
-def fill_slots(normed_rows, slot_ids, expert_count, capacity, choose_count):
-    targets = jnp.arange(expert_count * capacity, dtype=jnp.int32)
-    matched = (targets[:, None] == slot_ids[None, :]).astype(jnp.bfloat16)
-    repeated = jnp.repeat(normed_rows, choose_count, axis=0)
-    filled = jnp.dot(matched, repeated, preferred_element_type=jnp.float32).astype(jnp.bfloat16)
-    return filled.reshape(expert_count, capacity, normed_rows.shape[1])
+MESH = pl.DeviceIdType.MESH
+CORES = 2
+
+
+def round_up(value, unit):
+    return (value + unit - 1) // unit * unit
+
+
+def place():
+    tp = lax.axis_index("tp")
+    return lax.axis_index("sp"), tp // CORES, lax.rem(tp, CORES)
+
+
+def partner_of(sp, d, n_sp):
+    if n_sp & (n_sp - 1):
+        return lax.rem(sp + d, n_sp)
+    total, bit = 0, 1
+    while bit < n_sp:
+        total = total + lax.rem(sp // bit + d // bit, 2) * bit
+        bit *= 2
+    return total
+
+
+def source_of(sp, d, n_sp):
+    if n_sp & (n_sp - 1):
+        return lax.rem(sp + n_sp - d, n_sp)
+    return partner_of(sp, d, n_sp)
+
+
+def greet(n_sp, nz, sp, z, c):
+    barrier = pltpu.get_barrier_semaphore()
+    tp = z * CORES + c
+    for d in range(1, n_sp):
+        pl.semaphore_signal(
+            barrier, inc=1, device_id=(partner_of(sp, d, n_sp), tp), device_id_type=MESH
+        )
+    pl.semaphore_signal(
+        barrier, inc=1, device_id=(sp, z * CORES + 1 - c), device_id_type=MESH
+    )
+
+    @pl.when(z > 0)
+    def _():
+        pl.semaphore_signal(barrier, inc=1, device_id=(sp, tp - CORES), device_id_type=MESH)
+
+    @pl.when(z < nz - 1)
+    def _():
+        pl.semaphore_signal(barrier, inc=1, device_id=(sp, tp + CORES), device_id_type=MESH)
+
+    beside = jnp.where(z > 0, 1, 0) + jnp.where(z < nz - 1, 1, 0)
+    pl.semaphore_wait(barrier, n_sp + beside)
+
+
+def send(src, dst, send_sem, recv_sem, device):
+    return pltpu.make_async_remote_copy(
+        src_ref=src,
+        dst_ref=dst,
+        send_sem=send_sem,
+        recv_sem=recv_sem,
+        device_id=device,
+        device_id_type=MESH,
+    )
+
+
+def nearest_first(z, nz, visit):
+    def step(j, carry):
+        away = j // 2 + 1
+        behind = lax.rem(j, 2)
+        block = z + away * (1 - 2 * behind)
+
+        @pl.when((block >= 0) & (block < nz))
+        def _():
+            visit(block, behind)
+
+        return carry
+
+    lax.fori_loop(0, 2 * (nz - 1), step, 0)
+
+
+def farthest_first(z, nz, visit):
+    def step(j, carry):
+        away = nz - 1 - j // 2
+        behind = lax.rem(j, 2)
+        block = z + away * (1 - 2 * behind)
+
+        @pl.when((block >= 0) & (block < nz))
+        def _():
+            visit(block, behind)
+
+        return carry
+
+    lax.fori_loop(0, 2 * (nz - 1), step, 0)
+
+
+def dispatch_kernel(
+    n_sp, nz, normed, onehot, gate, up, hid, toks, comp, rows,
+    up_s, up_r, dn_s, dn_r, x_s, x_r, p_s, p_r,
+):
+    sp, z, c = place()
+    tp = z * CORES + c
+    peer_core = (sp, z * CORES + 1 - c)
+    above = (sp, lax.rem(z + 1, nz) * CORES + c)
+    below = (sp, lax.rem(z + nz - 1, nz) * CORES + c)
+    capp, width = comp.shape[2], comp.shape[3]
+    greet(n_sp, nz, sp, z, c)
+
+    def to_above(block, src):
+        return send(src, toks.at[block], up_s.at[block], up_r.at[block], above)
+
+    def to_below(block, src):
+        return send(src, toks.at[block], dn_s.at[block], dn_r.at[block], below)
+
+    def to_expert(block, d):
+        e = partner_of(sp, d, n_sp)
+        return send(
+            comp.at[block, e], rows.at[block, c, sp],
+            x_s.at[block, d], x_r.at[block, d], (e, tp),
+        )
+
+    def from_expert(block, d):
+        e = source_of(sp, d, n_sp)
+        return send(
+            comp.at[block, e], rows.at[block, c, e],
+            x_s.at[block, d], x_r.at[block, d], (e, tp),
+        )
+
+    def to_core(block, d):
+        e = source_of(sp, d, n_sp)
+        return send(
+            rows.at[block, c, e], rows.at[block, c, e],
+            p_s.at[block, d], p_r.at[block, d], peer_core,
+        )
+
+    def from_core(block, d):
+        e = source_of(sp, d, n_sp)
+        return send(
+            rows.at[block, 1 - c, e], rows.at[block, 1 - c, e],
+            p_s.at[block, d], p_r.at[block, d], peer_core,
+        )
+
+    def own_to_core(block):
+        return send(
+            comp.at[block, sp], rows.at[block, c, sp],
+            p_s.at[block, 0], p_r.at[block, 0], peer_core,
+        )
+
+    def deal(block, src):
+        def one(e, carry):
+            comp[block, e] = jnp.dot(
+                onehot[block, pl.ds(pl.multiple_of(e * capp, capp), capp), :],
+                src[...],
+                preferred_element_type=jnp.float32,
+            ).astype(jnp.bfloat16)
+            return carry
+
+        lax.fori_loop(0, n_sp, one, 0)
+        for d in range(1, n_sp):
+            to_expert(block, d).start()
+        own_to_core(block).start()
+        rows[block, c, sp] = comp[block, sp]
+
+    @pl.when(z < nz - 1)
+    def _():
+        to_above(z, normed).start()
+
+    @pl.when(z > 0)
+    def _():
+        to_below(z, normed).start()
+
+    deal(z, normed)
+
+    def gather(block, behind):
+        @pl.when(behind == 1)
+        def _():
+            to_above(block, toks.at[block]).wait_recv()
+
+            @pl.when(z < nz - 1)
+            def _():
+                to_above(block, toks.at[block]).start()
+
+        @pl.when(behind == 0)
+        def _():
+            to_below(block, toks.at[block]).wait_recv()
+
+            @pl.when(z > 0)
+            def _():
+                to_below(block, toks.at[block]).start()
+
+        deal(block, toks.at[block])
+
+    nearest_first(z, nz, gather)
+
+    def units(block, lane):
+        tile = rows[block, lane].reshape(n_sp * capp, width)
+        gate_pre = jnp.dot(tile, gate[...], preferred_element_type=jnp.float32)
+        upward = jnp.dot(tile, up[...], preferred_element_type=jnp.float32)
+        capped = jnp.minimum(gate_pre, clamp_limit)
+        linear = jnp.clip(upward, -clamp_limit, clamp_limit)
+        gated = capped * jax.nn.sigmoid(sigmoid_alpha * capped)
+        hid[block, lane] = (gated * (linear + 1.0)).astype(jnp.bfloat16)
+
+    def serve(block, behind):
+        for d in range(1, n_sp):
+            from_expert(block, d).wait_recv()
+            to_core(block, d).start()
+
+        def both(i, carry):
+            @pl.when(i == 1)
+            def _():
+                for d in range(n_sp):
+                    from_core(block, d).wait_recv()
+
+            units(block, lax.rem(c + i, CORES))
+            return carry
+
+        lax.fori_loop(0, CORES, both, 0)
+        for d in range(1, n_sp):
+            to_expert(block, d).wait_send()
+            to_core(block, d).wait_send()
+        own_to_core(block).wait_send()
+
+    serve(z, 0)
+    nearest_first(z, nz, serve)
+
+    @pl.when(z < nz - 1)
+    def _():
+        to_above(z, normed).wait_send()
+
+    @pl.when(z > 0)
+    def _():
+        to_below(z, normed).wait_send()
+
+    def drain(block, behind):
+        @pl.when((behind == 1) & (z < nz - 1))
+        def _():
+            to_above(block, toks.at[block]).wait_send()
+
+        @pl.when((behind == 0) & (z > 0))
+        def _():
+            to_below(block, toks.at[block]).wait_send()
+
+    nearest_first(z, nz, drain)
+
+
+def return_kernel(
+    n_sp, nz, tile_cols, hid, down, share_hi, share_lo, stream, out,
+    p_out, p_in, sums, back, a_out, a_up, a_dn,
+    up_s, up_r, dn_s, dn_r, x_s, x_r, p_s, p_r,
+):
+    sp, z, c = place()
+    tp = z * CORES + c
+    peer_core = (sp, z * CORES + 1 - c)
+    above = (sp, lax.rem(z + 1, nz) * CORES + c)
+    below = (sp, lax.rem(z + nz - 1, nz) * CORES + c)
+    capp, width = sums.shape[2], sums.shape[3]
+    col_tiles = width // tile_cols
+    greet(n_sp, nz, sp, z, c)
+
+    def cols_of(t):
+        return pl.ds(pl.multiple_of(t * tile_cols, tile_cols), tile_cols)
+
+    def to_core(block):
+        return send(p_out.at[block], p_in.at[block], p_s.at[block], p_r.at[block], peer_core)
+
+    def to_home(block, d):
+        e = partner_of(sp, d, n_sp)
+        return send(
+            sums.at[block, e], back.at[block, sp],
+            x_s.at[block, d], x_r.at[block, d], (e, tp),
+        )
+
+    def from_home(block, d):
+        e = source_of(sp, d, n_sp)
+        return send(
+            sums.at[block, e], back.at[block, e],
+            x_s.at[block, d], x_r.at[block, d], (e, tp),
+        )
+
+    def to_above(block):
+        return send(a_out.at[block], a_up.at[block], up_s.at[block], up_r.at[block], above)
+
+    def to_below(block):
+        return send(a_out.at[block], a_dn.at[block], dn_s.at[block], dn_r.at[block], below)
+
+    def lend(block, behind):
+        def one(t, carry):
+            cols = cols_of(t)
+            p_out[block, :, cols] = jnp.dot(
+                hid[block, 1 - c], down[:, cols], preferred_element_type=jnp.float32
+            ).astype(jnp.bfloat16)
+            return carry
+
+        lax.fori_loop(0, col_tiles, one, 0)
+        to_core(block).start()
+
+    def push(block, behind):
+        to_core(block).wait_recv()
+
+        def one(t, carry):
+            cols = cols_of(t)
+            part = jnp.dot(hid[block, c], down[:, cols], preferred_element_type=jnp.float32)
+            both = (part + p_in[block, :, cols].astype(jnp.float32)).astype(jnp.bfloat16)
+            sums[block, :, :, cols] = both.reshape(n_sp, capp, tile_cols)
+            return carry
+
+        lax.fori_loop(0, col_tiles, one, 0)
+        for d in range(1, n_sp):
+            to_home(block, d).start()
+        back[block, sp] = sums[block, sp]
+
+    def combined(block, cols):
+        picked = back[block, :, :, cols].reshape(n_sp * capp, tile_cols)
+        return jnp.dot(share_hi[block], picked, preferred_element_type=jnp.float32) + jnp.dot(
+            share_lo[block], picked, preferred_element_type=jnp.float32
+        )
+
+    def await_home(block):
+        for d in range(1, n_sp):
+            from_home(block, d).wait_recv()
+
+    def relay(block, behind):
+        await_home(block)
+
+        @pl.when(behind == 0)
+        def _():
+            @pl.when(z > 0)
+            def _():
+                to_above(block).wait_recv()
+
+            def one(t, carry):
+                cols = cols_of(t)
+                total = combined(block, cols)
+                total = jnp.where(z > 0, total + a_up[block, :, cols].astype(jnp.float32), total)
+                a_out[block, :, cols] = total.astype(jnp.bfloat16)
+                return carry
+
+            lax.fori_loop(0, col_tiles, one, 0)
+            to_above(block).start()
+
+        @pl.when(behind == 1)
+        def _():
+            @pl.when(z < nz - 1)
+            def _():
+                to_below(block).wait_recv()
+
+            def one(t, carry):
+                cols = cols_of(t)
+                total = combined(block, cols)
+                total = jnp.where(
+                    z < nz - 1, total + a_dn[block, :, cols].astype(jnp.float32), total
+                )
+                a_out[block, :, cols] = total.astype(jnp.bfloat16)
+                return carry
+
+            lax.fori_loop(0, col_tiles, one, 0)
+            to_below(block).start()
+
+    farthest_first(z, nz, lend)
+    lend(z, 0)
+    farthest_first(z, nz, push)
+    push(z, 0)
+    farthest_first(z, nz, relay)
+    await_home(z)
+
+    @pl.when(z > 0)
+    def _():
+        to_above(z).wait_recv()
+
+    @pl.when(z < nz - 1)
+    def _():
+        to_below(z).wait_recv()
+
+    def final(t, carry):
+        cols = cols_of(t)
+        total = combined(z, cols)
+        total = jnp.where(z > 0, total + a_up[z, :, cols].astype(jnp.float32), total)
+        total = jnp.where(z < nz - 1, total + a_dn[z, :, cols].astype(jnp.float32), total)
+        out[:, cols] = (stream[:, cols].astype(jnp.float32) + total).astype(jnp.bfloat16)
+        return carry
+
+    lax.fori_loop(0, col_tiles, final, 0)
+
+    def drain(block, behind):
+        to_core(block).wait_send()
+        for d in range(1, n_sp):
+            to_home(block, d).wait_send()
+
+    def drain_line(block, behind):
+        drain(block, behind)
+
+        @pl.when(behind == 0)
+        def _():
+            to_above(block).wait_send()
+
+        @pl.when(behind == 1)
+        def _():
+            to_below(block).wait_send()
+
+    drain(z, 0)
+    farthest_first(z, nz, drain_line)
+
+
+def experts(normed, stream, routes, route_weight, gate_local, up_local, down_local, capacity):
+    n_sp = lax.axis_size("sp")
+    n_tp = lax.axis_size("tp")
+    nz = n_tp // CORES
+    tok, width = normed.shape
+    units = gate_local.shape[1]
+    choose = routes.shape[1]
+    capp = round_up(capacity, 16)
+    slots = n_sp * capp
+    core = lax.rem(lax.axis_index("tp"), CORES)
+    lane_routes = lax.dynamic_index_in_dim(
+        routes.reshape(nz, CORES, tok, choose), core, 1, keepdims=False
+    )
+    ids = lane_routes.transpose(0, 2, 1)
+    named = (ids[:, :, None, :] == jnp.arange(n_sp, dtype=jnp.int32)[None, None, :, None])
+    member = jnp.any(named, axis=1)
+    earlier = jnp.arange(tok)[:, None] < jnp.arange(tok)[None, :]
+    rank = jnp.einsum(
+        "zet,tu->zeu",
+        member.astype(jnp.bfloat16),
+        earlier.astype(jnp.bfloat16),
+        preferred_element_type=jnp.float32,
+    )
+    own_rank = jnp.sum(jnp.where(named, rank[:, None], 0.0), axis=2).astype(jnp.int32)
+    slot = ids * capp + own_rank
+    places = jnp.arange(slots, dtype=jnp.int32)
+    onehot = jnp.any(slot[:, :, None, :] == places[None, None, :, None], axis=1).astype(jnp.bfloat16)
+    all_weight = lax.all_gather(route_weight, "tp", axis=0, tiled=False)
+    lane_weight = lax.dynamic_index_in_dim(
+        all_weight.reshape(nz, CORES, tok, choose), core, 1, keepdims=False
+    )
+    slot_t = slot.transpose(0, 2, 1)
+    share = jnp.sum(
+        jnp.where(
+            slot_t[:, :, :, None] == places[None, None, None, :], lane_weight[:, :, :, None], 0.0
+        ),
+        axis=2,
+    )
+    share_hi = share.astype(jnp.bfloat16)
+    share_lo = (share - share_hi.astype(jnp.float32)).astype(jnp.bfloat16)
+    vmem = pl.BlockSpec(memory_space=pltpu.VMEM)
+    dma = pltpu.SemaphoreType.DMA
+    bf = jnp.bfloat16
+    line = [dma((nz,))] * 4
+    hid = pl.pallas_call(
+        functools.partial(dispatch_kernel, n_sp, nz),
+        out_shape=jax.ShapeDtypeStruct((nz, CORES, slots, units), bf),
+        in_specs=[vmem] * 4,
+        out_specs=vmem,
+        scratch_shapes=[
+            pltpu.VMEM((nz, tok, width), bf),
+            pltpu.VMEM((nz, n_sp, capp, width), bf),
+            pltpu.VMEM((nz, CORES, n_sp, capp, width), bf),
+        ]
+        + line
+        + [dma((nz, n_sp))] * 4,
+        compiler_params=pltpu.CompilerParams(
+            collective_id=0, has_side_effects=True, vmem_limit_bytes=58 * 1024 * 1024
+        ),
+        name="dispatch",
+    )(normed, onehot, gate_local, up_local)
+    return pl.pallas_call(
+        functools.partial(return_kernel, n_sp, nz, min(512, width)),
+        out_shape=jax.ShapeDtypeStruct((tok, width), bf),
+        in_specs=[vmem] * 5,
+        out_specs=vmem,
+        scratch_shapes=[
+            pltpu.VMEM((nz, slots, width), bf),
+            pltpu.VMEM((nz, slots, width), bf),
+            pltpu.VMEM((nz, n_sp, capp, width), bf),
+            pltpu.VMEM((nz, n_sp, capp, width), bf),
+            pltpu.VMEM((nz, tok, width), bf),
+            pltpu.VMEM((nz, tok, width), bf),
+            pltpu.VMEM((nz, tok, width), bf),
+        ]
+        + line
+        + [dma((nz, n_sp))] * 2
+        + [dma((nz,))] * 2,
+        compiler_params=pltpu.CompilerParams(
+            collective_id=1, has_side_effects=True, vmem_limit_bytes=62 * 1024 * 1024
+        ),
+        name="give_back",
+    )(hid, down_local, share_hi, share_lo, stream)
 
 
 def local(
@@ -108,32 +572,9 @@
     ).astype(jnp.bfloat16)
     choose_count = routes.shape[1]
     capacity = max(2, 5 * tok_rows * choose_count // (4 * sp_count))
-    model_width = normed.shape[1]
-    gate_local = gate_weight[0]
-    up_local = up_weight[0]
-    down_local = down_weight[0]
-    own_routes = lax.dynamic_slice_in_dim(routes, tp_index * tok_rows, tok_rows, 0)
-    own_slots = slot_layout(own_routes, sp_count, capacity)
-    outgoing = fill_slots(normed, own_slots, sp_count, capacity, choose_count)
-    arrived = lax.all_to_all(outgoing, "sp", split_axis=0, concat_axis=0, tiled=True)
-    hidden = expert_hidden(
-        lax.all_gather(arrived[None], "tp", axis=0, tiled=True).reshape(-1, model_width),
-        gate_local,
-        up_local,
-    )
-    summed = lax.psum_scatter(
-        jnp.dot(hidden, down_local, preferred_element_type=jnp.float32).astype(jnp.bfloat16),
-        "tp",
-        scatter_dimension=0,
-        tiled=True,
-    )
-    expert_out = summed.reshape(sp_count, capacity, model_width)
-    returned = lax.all_to_all(expert_out, "sp", split_axis=0, concat_axis=0, tiled=True)
-    picked = returned.reshape(-1, model_width)[own_slots].reshape(
-        tok_rows, choose_count, model_width
-    )
-    combined = jnp.sum(picked.astype(jnp.float32) * route_weight[:, :, None], axis=1)
-    return (stream32 + combined).astype(jnp.bfloat16)
+    return experts(
+        normed, stream, routes, route_weight, gate_weight[0], up_weight[0], down_weight[0], capacity
+    )
 
 
 def solution(mesh):

time: 354 us -> 204 us (0.58)
  waiting for transfers between devices: 232 us -> 12.5 us
  Pallas kernels: 0 us -> 137 us
  matrix products: 36.5 us -> 10 us
  between operations: 13.7 us -> 0.36 us
  local copies, waits for them, and re-layouts: 24.2 us -> 14.7 us
  blocking collectives: 20.1 us -> 12.2 us
  starting transfers between devices: 17.1 us -> 11.9 us
  other arithmetic: 9.63 us -> 4.85 us
    pallas_call x0 -> x2, Pallas kernels: none -> 137 us  [the longest x1 71.1 us: experts(): pl.pallas_call(functools.partial(return_kernel, n_sp, nz, min(512, width)...]
    reduce_scatter x1 -> x0, waiting for transfers between devices: 108 us -> none  [local(): lax.psum_scatter(jnp.dot(hidden, down_local, preferred_element_type=jnp.f...]
    all_gather x1 -> x0, waiting for transfers between devices: 97.2 us -> none  [local(): lax.all_gather(arrived[None], 'tp', axis=0, tiled=True)]
    dot_general x3 -> x1, matrix products: 25.3 us -> 0.14 us  [experts(): jnp.einsum('zet,tu->zeu', member.astype(jnp.bfloat16), earlier.astype(jnp...]
    all_to_all x1 -> x0, blocking collectives: 20.1 us -> none  [local(): lax.all_to_all(outgoing, 'sp', split_axis=0, concat_axis=0, tiled=True)]
    all_to_all x1 -> x0, waiting for transfers between devices: 14.2 us -> none  [local(): lax.all_to_all(expert_out, 'sp', split_axis=0, concat_axis=0, tiled=True)]
    all_gather x0 -> x1, blocking collectives: none -> 12.2 us  [experts(): all_weight = lax.all_gather(route_weight, 'tp', axis=0, tiled=False)]
    reduce_sum x2, other arithmetic: 4.84 us -> 0.21 us  [the longest x1 0.18 us: experts(): jnp.sum(jnp.where(slot_t[:, :, :, None] == places[None, None, None, :], l...]
  transfers between devices with their start and end apart: 6 -> 3, of which waited for: 4 -> 1; matrix products, arithmetic and copies ran while one was open for 5% -> 7% of each run, Pallas kernels for 0% -> 0%
where the time goes in v1:
time: 204 us
  Pallas kernels  137 us (67%)
  local copies, waits for them, and re-layouts  14.7 us (7%)
  waiting for transfers between devices  12.5 us (6%)
  blocking collectives  12.2 us (6%)
  starting transfers between devices  11.9 us (6%)
  matrix products  10 us (5%)
  other arithmetic  4.85 us (2%)
    pallas_call x1, Pallas kernels, experts(): pl.pallas_call(functools.partial(return_kernel, n_sp, nz, min(512, width)...  71.1 us
    pallas_call x1, Pallas kernels, experts(): pl.pallas_call(functools.partial(dispatch_kernel, n_sp, nz), out_shape=ja...  65.8 us
    all_to_all x1, waiting for transfers between devices, local(): lax.all_to_all(attended, 'tp', split_axis=0, concat_axis=1, tiled=True)  12.5 us
    all_gather x1, blocking collectives, experts(): all_weight = lax.all_gather(route_weight, 'tp', axis=0, tiled=False)  12.2 us
    ppermute x2, starting transfers between devices, from_behind(): return lax.ppermute(block, axis, route)  8.25 us
    dot_general x1, matrix products, local(): mixed = jnp.dot(token_heads, out_weight, preferred_element_type=jnp.float32)  4.77 us
    dot_general x1, matrix products, local(): jnp.einsum('nhgqk,nkhd->nqhgd', weights_bf, value_band, preferred_element...  4.18 us
  transfers between devices with their start and end apart: 3, of which 1 were waited for; matrix products, arithmetic and copies ran while one was open for 7% of the time, Pallas kernels for 0%

profile of v1, /device:TPU:0, one launch (start us, length us, event | category | flops | bytes accessed | tf_op | source)
XLA Modules:
  0.0 203.6 jit_solution(14315253824265655443)
XLA Ops:
  0.0 0.0 slice-start
  0.0 0.0 slice-start.1
  0.0 0.0 copy-start.5
  0.0 0.8 slice.21
  0.8 4.9 %collective-permute-start.1 = (bf16[128,128]{1,0:T(8,128)(2,1)S(1)}, bf16[128,128]{1,0:T(8,128)(2,1)S(1)}, u32[]{:S(2)}, u32[]{:S(2)}) collective-permute-start(bf16[128,128]{1,0:T(8,128)(2,1)S(1)} %slice.21), channel_id=1, source_target_pairs={{0,8},{8,16},{16,24},{1,9},{9,17},{17,25},{2,10},{10,18},{18,26},{... | collective-permute-start | bytes 98312 | tf_op jit(solution)/shard_map/ppermute | solution.py:22
  5.7 0.8 slice.18
  6.5 3.4 %collective-permute-start = (bf16[128,128]{1,0:T(8,128)(2,1)S(1)}, bf16[128,128]{1,0:T(8,128)(2,1)S(1)}, u32[]{:S(2)}, u32[]{:S(2)}) collective-permute-start(bf16[128,128]{1,0:T(8,128)(2,1)S(1)} %slice.18), channel_id=1, source_target_pairs={{0,8},{8,16},{16,24},{1,9},{9,17},{17,25},{2,10},{10,18},{18,26},{... | collective-permute-start | bytes 98312 | tf_op jit(solution)/shard_map/ppermute | solution.py:22
  9.9 0.1 add_compare_fusion
  10.0 0.7 reshape.129
  10.8 0.1 fusion.23
  11.0 12.2 %all-gather = f32[1024,2]{0,1:T(2,128)S(1)} all-gather(f32[128,2]{0,1:T(2,128)} %param.20), channel_id=2, replica_groups=mesh['sp'=4,'tp'=8] {'tp'}, dimensions={0}, use_global_device_ids=true | all-gather | bytes 9216 | tf_op jit(solution)/shard_map/all_gather | solution.py:453
  23.2 0.3 broadcast_and_fusion
  23.6 1.2 reshape.139
  24.8 1.2 reshape.137
  26.0 2.5 %reshape.140 = bf16[8,128,2,2,64]{4,3,2,1,0:T(2,128)(2,1)S(1)} reshape(bf16[1024,256]{1,0:T(8,128)(2,1)} %param.12) | data formatting | bytes 1048576 | tf_op jit(solution)/shard_map/reshape | solution.py:541
  28.5 0.4 copy.69
  28.9 0.0 slice-done
  28.9 0.2 reshape.138
  29.1 0.9 copy.67
  30.0 0.0 copy-done.5
  30.0 0.1 max.18
  30.1 0.3 copy.64
  30.5 0.0 slice-done.1
  30.5 0.2 reshape.136
  30.7 0.9 copy.62
  31.6 0.0 collective-permute-done.1
  31.6 0.1 copy.65
  31.8 0.9 fusion.1
  32.7 0.0 copy-start.1
  32.7 0.1 broadcast_maximum_fusion
  32.8 1.8 copy-done.1
  34.6 1.0 fusion
  35.6 0.1 exponential_add_fusion
  35.7 0.0 collective-permute-done
  35.7 0.1 copy.60
  35.9 4.2 %fusion.5 = bf16[8,2,64,2,128]{4,2,3,1,0:T(8,128)(2,1)} fusion(f32[8,2,256,128,2]{3,2,4,1,0:T(8,128)} %copy-done.1, f32[8,2,2,128]{3,2,1,0:T(2,128)S(1)} %exponential_add_fusion, f32[8,2,2,128]{3,2,1,0:T(2,128)S(1)} %broadcast_maximum_fusion, pred[8,128,256]{1,2,0:T(8,128)(4,1)S(1)} %broadcast_and_fusion, bf16[8,128,2,64]{1,3,2,0:T(8,128)(2,1)S(1)} %copy.64, ...), kind=kOutput, calls=%fused_computation.14 | convolution fusion | flops 141295616 | bytes 5537792 | tf_op jit(solution)/shard_map/nhgqk,nkhd->nqhgd/dot_general | solution.py:558
  40.0 0.0 copy-start.3
  40.0 3.6 %all-to-all-start = ((bf16[8,128,256]{1,2,0:T(8,128)(2,1)}), bf16[8,128,256]{1,2,0:T(8,128)(2,1)S(1)}, u32[]{:S(2)}, u32[]{:S(2)}) async-start(bf16[8,128,256]{1,2,0:T(8,128)(2,1)} %bitcast.8), calls=%async_computation | async-start | bytes 1048576 | tf_op jit(solution)/shard_map/all_to_all | solution.py:564
  43.7 0.2 select_reduce_fusion
  43.9 0.3 copy.79
  44.2 0.2 fusion.4
  44.5 0.8 convert_element_type.50.onehot
  45.3 0.2 copy.80.share_hi
  45.5 0.0 copy-start.2
  45.5 0.9 subtract_convert_fusion.share_lo
  46.4 12.5 %all-to-all-done = bf16[8,128,256]{1,2,0:T(8,128)(2,1)S(1)} async-done(((bf16[8,128,256]{1,2,0:T(8,128)(2,1)}), bf16[8,128,256]{1,2,0:T(8,128)(2,1)S(1)}, u32[]{:S(2)}, u32[]{:S(2)}) %all-to-all-start) | async-done | bytes 524320 | tf_op jit(solution)/shard_map/all_to_all | solution.py:564
  58.9 0.0 copy-done.3
  58.9 0.0 copy-start.4
  58.9 4.8 %fusion.6 = (f32[128]{0:T(128)S(1)}, bf16[128,2048]{1,0:T(8,128)(2,1)S(1)}) fusion(bf16[128,2048]{0,1:T(8,128)(2,1)S(1)} %bitcast.57, bf16[2048,2048]{1,0:T(8,128)(2,1)} %param.17, bf16[128,2048]{1,0:T(8,128)(2,1)S(1)} %copy-done.3), kind=kOutput, calls=%fused_computation.15 | convolution fusion | flops 1075314560 | bytes 9961984 | tf_op jit(solution)/shard_map/dot_general | solution.py:565
  63.7 0.0 copy-done.2
  63.7 0.0 copy-start
  63.7 0.0 copy-done.4
  63.8 1.0 fusion.8.normed
  64.7 65.8 %dispatch.1.hid = bf16[4,2,320,256]{3,2,1,0:T(8,128)(2,1)} custom-call(bf16[128,2048]{1,0:T(8,128)(2,1)} %fusion.8.normed, bf16[4,320,128]{2,1,0:T(8,128)(2,1)} %convert_element_type.50.onehot, bf16[2048,256]{1,0:T(8,128)(2,1)} %bitcast.58, bf16[2048,256]{1,0:T(8,128)(2,1)} %bitcast.59), custom_call_target="tpu_custom_call" | custom-call | tf_op jit(solution)/shard_map/dispatch/pallas_call | solution.py:470
  130.5 0.0 copy-done
  130.6 71.1 %give_back.1 = bf16[128,2048]{1,0:T(8,128)(2,1)} custom-call(bf16[4,2,320,256]{3,2,1,0:T(8,128)(2,1)} %dispatch.1.hid, bf16[256,2048]{1,0:T(8,128)(2,1)} %bitcast.60, bf16[4,128,320]{2,1,0:T(8,128)(2,1)} %copy-done.2, bf16[4,128,320]{2,1,0:T(8,128)(2,1)} %subtract_convert_fusion.share_lo, bf16[128,2048]{1,0:T(8,128)(2,1)} %copy-done), custom_call_target="tpu_custom_call" | custom-call | tf_op jit(solution)/shard_map/give_back/pallas_call | solution.py:487
  201.7 1.9 copy.106
  (14 shorter events, 0.2 us)
Async XLA Ops:
  0.0 28.9 %slice-start = ((bf16[1024,128]{1,0:T(8,128)(2,1)}), bf16[896,128]{1,0:T(8,128)(2,1)S(1)}, s32[]{:S(2)}) async-start(bf16[1024,128]{1,0:T(8,128)(2,1)} %param.13), calls=%async_computation.1 | async-start | bytes 458752 | tf_op jit(solution)/shard_map/slice | solution.py:536
  0.0 30.5 %slice-start.1 = ((bf16[1024,128]{1,0:T(8,128)(2,1)}), bf16[896,128]{1,0:T(8,128)(2,1)S(1)}, s32[]{:S(2)}) async-start(bf16[1024,128]{1,0:T(8,128)(2,1)} %param.14), calls=%async_computation.2 | async-start | bytes 458752 | tf_op jit(solution)/shard_map/slice | solution.py:536
  0.0 30.0 %copy-start.5 = (f32[4]{0:T(128)S(1)}, f32[4]{0:T(128)}, u32[]{:S(2)}) copy-start(f32[4]{0:T(128)} %param.15) | copy-start | bytes 52
  0.8 30.8 %collective-permute-start.1 = (bf16[128,128]{1,0:T(8,128)(2,1)S(1)}, bf16[128,128]{1,0:T(8,128)(2,1)S(1)}, u32[]{:S(2)}, u32[]{:S(2)}) collective-permute-start(bf16[128,128]{1,0:T(8,128)(2,1)S(1)} %slice.21), channel_id=1, source_target_pairs={{0,8},{8,16},{16,24},{1,9},{9,17},{17,25},{2,10},{10,18},{18,26},{... | collective-permute-start | bytes 98312 | tf_op jit(solution)/shard_map/ppermute | solution.py:22
  6.5 29.3 %collective-permute-start = (bf16[128,128]{1,0:T(8,128)(2,1)S(1)}, bf16[128,128]{1,0:T(8,128)(2,1)S(1)}, u32[]{:S(2)}, u32[]{:S(2)}) collective-permute-start(bf16[128,128]{1,0:T(8,128)(2,1)S(1)} %slice.18), channel_id=1, source_target_pairs={{0,8},{8,16},{16,24},{1,9},{9,17},{17,25},{2,10},{10,18},{18,26},{... | collective-permute-start | bytes 98312 | tf_op jit(solution)/shard_map/ppermute | solution.py:22
  32.7 1.9 copy-start.1
  40.0 18.9 %copy-start.3 = (bf16[128,2048]{1,0:T(8,128)(2,1)S(1)}, bf16[128,2048]{1,0:T(8,128)(2,1)}, u32[]{:S(2)}) copy-start(bf16[128,2048]{1,0:T(8,128)(2,1)} %param.16) | copy-start | bytes 1572868
  40.0 18.9 %all-to-all-start = ((bf16[8,128,256]{1,2,0:T(8,128)(2,1)}), bf16[8,128,256]{1,2,0:T(8,128)(2,1)S(1)}, u32[]{:S(2)}, u32[]{:S(2)}) async-start(bf16[8,128,256]{1,2,0:T(8,128)(2,1)} %bitcast.8), calls=%async_computation | async-start | bytes 1048576 | tf_op jit(solution)/shard_map/all_to_all | solution.py:564
  45.5 18.2 %copy-start.2 = (bf16[4,128,320]{2,1,0:T(8,128)(2,1)}, bf16[4,128,320]{2,1,0:T(8,128)(2,1)S(1)}, u32[]{:S(2)}) copy-start(bf16[4,128,320]{2,1,0:T(8,128)(2,1)S(1)} %copy.80.share_hi) | copy-start | bytes 983044
  58.9 4.8 %copy-start.4 = (f32[2048]{0:T(1024)S(1)}, f32[2048]{0:T(1024)}, u32[]{:S(2)}) copy-start(f32[2048]{0:T(1024)} %param.18) | copy-start | bytes 24580
  63.7 66.8 %copy-start = (bf16[128,2048]{1,0:T(8,128)(2,1)}, bf16[128,2048]{1,0:T(8,128)(2,1)S(1)}, u32[]{:S(2)}) copy-start(bf16[128,2048]{1,0:T(8,128)(2,1)S(1)} %get-tuple-element.8.stream) | copy-start | bytes 1572868

commit v2 on v1

--- a/solution.py
+++ b/solution.py
@@ -16,14 +16,9 @@
 sigmoid_alpha = 1.702
 
 
-def from_behind(block, axis, distance):
-    devices = range(lax.axis_size(axis))
-    route = [(i - distance, i) for i in devices if i - distance in devices]
-    return lax.ppermute(block, axis, route)
-
-
 MESH = pl.DeviceIdType.MESH
 CORES = 2
+LANES = 128
 
 
 def round_up(value, unit):
@@ -116,7 +111,7 @@
 
 
 def dispatch_kernel(
-    n_sp, nz, normed, onehot, gate, up, hid, toks, comp, rows,
+    n_sp, nz, normed, onehot, gate, up, hid, shares, toks, comp, rows,
     up_s, up_r, dn_s, dn_r, x_s, x_r, p_s, p_r,
 ):
     sp, z, c = place()
@@ -168,10 +163,12 @@
         )
 
     def deal(block, src):
+        shares[block] = src[:, pl.ds(width, LANES)]
+
         def one(e, carry):
             comp[block, e] = jnp.dot(
                 onehot[block, pl.ds(pl.multiple_of(e * capp, capp), capp), :],
-                src[...],
+                src[:, pl.ds(0, width)],
                 preferred_element_type=jnp.float32,
             ).astype(jnp.bfloat16)
             return carry
@@ -450,30 +447,26 @@
     slot = ids * capp + own_rank
     places = jnp.arange(slots, dtype=jnp.int32)
     onehot = jnp.any(slot[:, :, None, :] == places[None, None, :, None], axis=1).astype(jnp.bfloat16)
-    all_weight = lax.all_gather(route_weight, "tp", axis=0, tiled=False)
-    lane_weight = lax.dynamic_index_in_dim(
-        all_weight.reshape(nz, CORES, tok, choose), core, 1, keepdims=False
-    )
-    slot_t = slot.transpose(0, 2, 1)
-    share = jnp.sum(
-        jnp.where(
-            slot_t[:, :, :, None] == places[None, None, None, :], lane_weight[:, :, :, None], 0.0
-        ),
-        axis=2,
-    )
-    share_hi = share.astype(jnp.bfloat16)
-    share_lo = (share - share_hi.astype(jnp.float32)).astype(jnp.bfloat16)
+    weight_hi = lax.reduce_precision(route_weight, 8, 7)
+    weight_mid = lax.reduce_precision(route_weight - weight_hi, 8, 7)
+    weight_lo = route_weight - weight_hi - weight_mid
+    carried = jnp.concatenate([weight_hi, weight_mid, weight_lo], axis=1)
+    carried = jnp.pad(carried, ((0, 0), (0, LANES - 3 * choose))).astype(jnp.bfloat16)
+    payload = jnp.concatenate([normed, carried], axis=1)
     vmem = pl.BlockSpec(memory_space=pltpu.VMEM)
     dma = pltpu.SemaphoreType.DMA
     bf = jnp.bfloat16
     line = [dma((nz,))] * 4
-    hid = pl.pallas_call(
+    hid, shares = pl.pallas_call(
         functools.partial(dispatch_kernel, n_sp, nz),
-        out_shape=jax.ShapeDtypeStruct((nz, CORES, slots, units), bf),
+        out_shape=(
+            jax.ShapeDtypeStruct((nz, CORES, slots, units), bf),
+            jax.ShapeDtypeStruct((nz, tok, LANES), bf),
+        ),
         in_specs=[vmem] * 4,
-        out_specs=vmem,
+        out_specs=(vmem, vmem),
         scratch_shapes=[
-            pltpu.VMEM((nz, tok, width), bf),
+            pltpu.VMEM((nz, tok, width + LANES), bf),
             pltpu.VMEM((nz, n_sp, capp, width), bf),
             pltpu.VMEM((nz, CORES, n_sp, capp, width), bf),
         ]
@@ -483,7 +476,21 @@
             collective_id=0, has_side_effects=True, vmem_limit_bytes=58 * 1024 * 1024
         ),
         name="dispatch",
-    )(normed, onehot, gate_local, up_local)
+    )(payload, onehot, gate_local, up_local)
+    parts = shares[:, :, : 3 * choose].astype(jnp.float32)
+    lane_weight = (
+        parts[:, :, :choose] + parts[:, :, choose : 2 * choose] + parts[:, :, 2 * choose :]
+    )
+    slot_t = slot.transpose(0, 2, 1)
+    share = jnp.sum(
+        jnp.where(
+            slot_t[:, :, :, None] == places[None, None, None, :], lane_weight[:, :, :, None], 0.0
+        ),
+        axis=2,
+    )
+    rounded = lax.reduce_precision(share, 8, 7)
+    share_hi = rounded.astype(jnp.bfloat16)
+    share_lo = (share - rounded).astype(jnp.bfloat16)
     return pl.pallas_call(
         functools.partial(return_kernel, n_sp, nz, min(512, width)),
         out_shape=jax.ShapeDtypeStruct((tok, width), bf),
@@ -508,6 +515,157 @@
     )(hid, down_local, share_hi, share_lo, stream)
 
 
+def attention_kernel(
+    n_sp, n_tp, tok, q, k, v, sink, out, k_all, v_all, k_tail, v_tail, att, got,
+    t_s, t_r, a_s, a_r,
+):
+    sp, tp = lax.axis_index("sp"), lax.axis_index("tp")
+    span, kv_cols = k.shape
+    cols = q.shape[1]
+    kv_local = kv_cols // HEAD
+    group = cols // kv_cols
+    blocks = span // WINDOW
+    pieces = WINDOW // tok
+    barrier = pltpu.get_barrier_semaphore()
+    for d in range(1, n_tp):
+        pl.semaphore_signal(
+            barrier, inc=1, device_id=(sp, lax.rem(tp + d, n_tp)), device_id_type=MESH
+        )
+
+    @pl.when(sp > 0)
+    def _():
+        pl.semaphore_signal(barrier, inc=1, device_id=(sp - 1, tp), device_id_type=MESH)
+
+    @pl.when(sp < n_sp - 1)
+    def _():
+        pl.semaphore_signal(barrier, inc=1, device_id=(sp + 1, tp), device_id_type=MESH)
+
+    beside = jnp.where(sp > 0, 1, 0) + jnp.where(sp < n_sp - 1, 1, 0)
+    pl.semaphore_wait(barrier, n_tp - 1 + beside)
+    ahead = (lax.rem(sp + 1, n_sp), tp)
+    last = pl.ds(span - WINDOW, WINDOW)
+    tails = (
+        send(k.at[last], k_tail, t_s.at[0], t_r.at[0], ahead),
+        send(v.at[last], v_tail, t_s.at[1], t_r.at[1], ahead),
+    )
+
+    @pl.when(sp < n_sp - 1)
+    def _():
+        for copy in tails:
+            copy.start()
+
+    k_all[pl.ds(WINDOW, span), :] = k[...]
+    v_all[pl.ds(WINDOW, span), :] = v[...]
+    row = lax.broadcasted_iota(jnp.int32, (WINDOW, 2 * WINDOW), 0)
+    col = lax.broadcasted_iota(jnp.int32, (WINDOW, 2 * WINDOW), 1)
+    distance = row + WINDOW - col
+    banded = (distance >= 0) & (distance < WINDOW)
+
+    def to_owner(dest):
+        at = pl.multiple_of(dest * tok, tok)
+        return send(
+            att.at[pl.ds(at, tok)], got.at[tp], a_s.at[dest], a_r.at[tp], (sp, dest)
+        )
+
+    def attend(i, carry):
+        block = lax.rem(tp // pieces + 1 + i, blocks)
+
+        @pl.when(block == 0)
+        def _():
+            @pl.when(sp > 0)
+            def _():
+                for copy in tails:
+                    copy.wait_recv()
+                k_all[pl.ds(0, WINDOW), :] = k_tail[...]
+                v_all[pl.ds(0, WINDOW), :] = v_tail[...]
+
+            @pl.when(sp == 0)
+            def _():
+                k_all[pl.ds(0, WINDOW), :] = jnp.zeros((WINDOW, kv_cols), jnp.bfloat16)
+                v_all[pl.ds(0, WINDOW), :] = jnp.zeros((WINDOW, kv_cols), jnp.bfloat16)
+
+        at = pl.multiple_of(block * WINDOW, WINDOW)
+        start = jnp.where((sp == 0) & (block == 0), WINDOW, 0)
+        allowed = banded & (col >= start)
+        band = pl.ds(at, 2 * WINDOW)
+        for g in range(kv_local):
+            keys = k_all[band, g * HEAD : (g + 1) * HEAD]
+            values = v_all[band, g * HEAD : (g + 1) * HEAD]
+            heads = []
+            for m in range(group):
+                h = g * group + m
+                query = q[pl.ds(at, WINDOW), h * HEAD : (h + 1) * HEAD]
+                scores = lax.dot_general(
+                    query, keys, (((1,), (1,)), ((), ())), preferred_element_type=jnp.float32
+                ) * HEAD ** (-0.5)
+                logits = jnp.where(allowed, scores, -jnp.inf)
+                top = jnp.maximum(jnp.max(logits, axis=-1, keepdims=True), sink[h])
+                raised = jnp.exp(logits - top)
+                total = jnp.sum(raised, axis=-1, keepdims=True) + jnp.exp(sink[h] - top)
+                probs = (raised / total).astype(jnp.bfloat16)
+                heads.append(jnp.dot(probs, values, preferred_element_type=jnp.float32))
+            att[pl.ds(at, WINDOW), g * group * HEAD : (g + 1) * group * HEAD] = jnp.concatenate(
+                heads, axis=1
+            ).astype(jnp.bfloat16)
+        for piece in range(pieces):
+            dest = block * pieces + piece
+
+            @pl.when(dest != tp)
+            def _():
+                to_owner(dest).start()
+
+        return carry
+
+    lax.fori_loop(0, blocks, attend, 0)
+    got[tp] = att[pl.ds(pl.multiple_of(tp * tok, tok), tok), :]
+    for p in range(n_tp):
+        @pl.when(tp != p)
+        def _():
+            send(att.at[pl.ds(0, tok)], got.at[p], a_s.at[p], a_r.at[p], (sp, p)).wait_recv()
+
+        out[:, p * cols : (p + 1) * cols] = got[p]
+    for p in range(n_tp):
+        @pl.when(tp != p)
+        def _():
+            to_owner(p).wait_send()
+
+    @pl.when(sp < n_sp - 1)
+    def _():
+        for copy in tails:
+            copy.wait_send()
+
+
+def attend_tokens(query_heads, key_heads, value_heads, sink_logit, tok):
+    n_sp, n_tp = lax.axis_size("sp"), lax.axis_size("tp")
+    span, cols = query_heads.shape
+    kv_cols = key_heads.shape[1]
+    vmem = pl.BlockSpec(memory_space=pltpu.VMEM)
+    dma = pltpu.SemaphoreType.DMA
+    bf = jnp.bfloat16
+    return pl.pallas_call(
+        functools.partial(attention_kernel, n_sp, n_tp, tok),
+        out_shape=jax.ShapeDtypeStruct((tok, n_tp * cols), bf),
+        in_specs=[vmem] * 3 + [pl.BlockSpec(memory_space=pltpu.SMEM)],
+        out_specs=vmem,
+        scratch_shapes=[
+            pltpu.VMEM((span + WINDOW, kv_cols), bf),
+            pltpu.VMEM((span + WINDOW, kv_cols), bf),
+            pltpu.VMEM((WINDOW, kv_cols), bf),
+            pltpu.VMEM((WINDOW, kv_cols), bf),
+            pltpu.VMEM((span, cols), bf),
+            pltpu.VMEM((n_tp, tok, cols), bf),
+            dma((2,)),
+            dma((2,)),
+            dma((n_tp,)),
+            dma((n_tp,)),
+        ],
+        compiler_params=pltpu.CompilerParams(
+            collective_id=2, has_side_effects=True, vmem_limit_bytes=24 * 1024 * 1024
+        ),
+        name="attend",
+    )(query_heads, key_heads, value_heads, sink_logit)
+
+
 def local(
     query_heads,
     key_heads,
@@ -523,45 +681,8 @@
     down_weight,
 ):
     sp_count = lax.axis_size("sp")
-    span_rows = query_heads.shape[0]
-    kv_local = key_heads.shape[1] // HEAD
-    group_size = query_heads.shape[1] // key_heads.shape[1]
-    block_count = span_rows // WINDOW
-    key_tail, value_tail = from_behind(
-        (key_heads[span_rows - WINDOW :], value_heads[span_rows - WINDOW :]), "sp", 1
-    )
-
-    def banded(current, tail):
-        shaped = current.reshape(block_count, WINDOW, kv_local, HEAD)
-        earlier = jnp.concatenate([tail.reshape(1, WINDOW, kv_local, HEAD), shaped[:-1]], axis=0)
-        return jnp.concatenate([earlier, shaped], axis=1)
-
-    key_band = banded(key_heads, key_tail)
-    value_band = banded(value_heads, value_tail)
-    query_blocks = query_heads.reshape(block_count, WINDOW, kv_local, group_size, HEAD)
-    scores = jnp.einsum(
-        "nqhgd,nkhd->nhgqk", query_blocks, key_band, preferred_element_type=jnp.float32
-    ) * HEAD ** (-0.5)
-    query_pos = jnp.arange(WINDOW)[:, None]
-    key_col = jnp.arange(2 * WINDOW)[None, :]
-    distance = query_pos + WINDOW - key_col
-    block_ids = jnp.arange(block_count)[:, None, None]
-    key_global = lax.axis_index("sp") * span_rows + (block_ids - 1) * WINDOW + key_col[None]
-    allowed = (distance[None] >= 0) & (distance[None] < WINDOW) & (key_global >= 0)
-    logits = jnp.where(allowed[:, None, None], scores, -jnp.inf)
-    sink_term = sink_logit.reshape(kv_local, group_size)[None, :, :, None, None]
-    row_max = jnp.maximum(jnp.max(logits, axis=-1, keepdims=True), sink_term)
-    raised = jnp.exp(logits - row_max)
-    weights_bf = (
-        raised / (jnp.sum(raised, axis=-1, keepdims=True) + jnp.exp(sink_term - row_max))
-    ).astype(jnp.bfloat16)
-    attended = jnp.einsum(
-        "nhgqk,nkhd->nqhgd", weights_bf, value_band, preferred_element_type=jnp.float32
-    )
-    attended = attended.astype(jnp.bfloat16).reshape(span_rows, query_heads.shape[1])
     tok_rows = residual.shape[0]
-    tp_index = lax.axis_index("tp")
-    token_heads = lax.all_to_all(attended, "tp", split_axis=0, concat_axis=1, tiled=True)
+    token_heads = attend_tokens(query_heads, key_heads, value_heads, sink_logit, tok_rows)
     mixed = jnp.dot(token_heads, out_weight, preferred_element_type=jnp.float32)
     stream = (residual.astype(jnp.float32) + mixed).astype(jnp.bfloat16)
     stream32 = stream.astype(jnp.float32)

time: 204 us -> 177 us (0.87)
  Pallas kernels: 137 us -> 159 us
  waiting for transfers between devices: 12.5 us -> 0 us
  blocking collectives: 12.2 us -> 0 us
  starting transfers between devices: 11.9 us -> 0 us
  local copies, waits for them, and re-layouts: 14.7 us -> 6.99 us
  matrix products: 10 us -> 4.95 us
    pallas_call x1 -> x2, Pallas kernels: 65.8 us -> 88.3 us  [the longest x1 70.8 us: experts(): pl.pallas_call(functools.partial(dispatch_kernel, n_sp, nz), out_shape=(j...]
    all_to_all x1 -> x0, waiting for transfers between devices: 12.5 us -> none  [local(): lax.all_to_all(attended, 'tp', split_axis=0, concat_axis=1, tiled=True)]
    all_gather x1 -> x0, blocking collectives: 12.2 us -> none  [experts(): all_weight = lax.all_gather(route_weight, 'tp', axis=0, tiled=False)]
    ppermute x2 -> x0, starting transfers between devices: 8.25 us -> none  [from_behind(): return lax.ppermute(block, axis, route)]
    reshape x6 -> x0, local copies, waits for them, and re-layouts: 5.61 us -> none  [the longest x4 3.08 us: banded(): shaped = current.reshape(block_count, WINDOW, kv_local, HEAD)]
    dot_general x2 -> x0, matrix products: 5.11 us -> none  [the longest x1 4.18 us: local(): jnp.einsum('nhgqk,nkhd->nqhgd', weights_bf, value_band, preferred_element...]
    slice x10 -> x0, local copies, waits for them, and re-layouts: 3.86 us -> none  [the longest x8 2.27 us: banded(): shaped[:-1]]
    all_to_all x1 -> x0, starting transfers between devices: 3.63 us -> none  [local(): lax.all_to_all(attended, 'tp', split_axis=0, concat_axis=1, tiled=True)]
  transfers between devices with their start and end apart: 3 -> 0, of which waited for: 1 -> 0; matrix products, arithmetic and copies ran while one was open for 7% -> 0% of each run, Pallas kernels for 0% -> 0%
where the time goes in v2:
time: 177 us; the launch traced here: 176 us
  Pallas kernels  159 us (90%)
  local copies, waits for them, and re-layouts  6.99 us (4%)
  other arithmetic  5.26 us (3%)
  matrix products  4.95 us (3%)
    pallas_call x1, Pallas kernels, experts(): pl.pallas_call(functools.partial(dispatch_kernel, n_sp, nz), out_shape=(j...  70.8 us
    pallas_call x1, Pallas kernels, experts(): pl.pallas_call(functools.partial(return_kernel, n_sp, nz, min(512, width)...  70.7 us
    pallas_call x1, Pallas kernels, attend_tokens(): pl.pallas_call(functools.partial(attention_kernel, n_sp, n_tp, tok), out_...  17.5 us
    unnamed x15, local copies, waits for them, and re-layouts  5.49 us
    dot_general x1, matrix products, local(): mixed = jnp.dot(token_heads, out_weight, preferred_element_type=jnp.float32)  4.81 us

profile of v2, /device:TPU:0, one launch (start us, length us, event | category | flops | bytes accessed | tf_op | source)
XLA Modules:
  0.0 176.4 jit_solution(5799980102327198390)
XLA Ops:
  0.0 0.0 copy-start.5
  0.0 0.7 reduce-precision_convert_fusion.1
  0.8 0.7 reshape.17
  1.5 0.1 fusion.8
  1.7 0.1 copy.37
  1.9 0.2 fusion.1
  2.1 0.8 convert_element_type.41.onehot
  2.9 0.0 copy-start
  2.9 1.0 copy-done
  3.9 0.0 copy-start.1
  3.9 0.9 copy-done.1
  4.9 0.0 copy-start.2
  4.9 0.9 copy-done.2
  5.8 0.0 copy-start.3
  5.8 0.7 copy-done.3
  6.5 17.5 %attend.1 = bf16[128,2048]{1,0:T(8,128)(2,1)S(1)} custom-call(bf16[1024,256]{1,0:T(8,128)(2,1)S(1)} %copy-done, bf16[1024,128]{1,0:T(8,128)(2,1)S(1)} %copy-done.1, bf16[1024,128]{1,0:T(8,128)(2,1)S(1)} %copy-done.2, f32[4]{0:T(128)S(1)} %copy-done.3), custom_call_target="tpu_custom_call" | custom-call | tf_op jit(solution)/shard_map/attend/pallas_call | solution.py:645
  24.0 0.0 copy-done.5
  24.0 0.0 copy-start.6
  24.0 4.8 %fusion.3 = (f32[128]{0:T(128)S(1)}, bf16[128,2048]{1,0:T(8,128)(2,1)S(1)}) fusion(bf16[128,2048]{1,0:T(8,128)(2,1)S(1)} %attend.1, bf16[2048,2048]{1,0:T(8,128)(2,1)} %param.17, bf16[128,2048]{1,0:T(8,128)(2,1)S(1)} %copy-done.5), kind=kOutput, calls=%fused_computation.10 | convolution fusion | flops 1075314560 | bytes 9961984 | tf_op jit(solution)/shard_map/dot_general | solution.py:686
  28.8 0.0 copy-start.4
  28.9 0.0 copy-done.6
  28.9 0.2 fusion.5
  29.1 0.9 fusion.6.normed
  29.9 70.8 %dispatch.1 = (bf16[4,2,320,256]{3,2,1,0:T(8,128)(2,1)}, bf16[4,128,128]{2,1,0:T(8,128)(2,1)}) custom-call(bf16[128,2176]{1,0:T(8,128)(2,1)} %fusion.6.normed, bf16[4,320,128]{2,1,0:T(8,128)(2,1)} %convert_element_type.41.onehot, bf16[2048,256]{1,0:T(8,128)(2,1)} %bitcast.21, bf16[2048,256]{1,0:T(8,128)(2,1)} %bitcast.22), custom_call_target="tpu_custom_call" | custom-call | tf_op jit(solution)/shard_map/dispatch/pallas_call | solution.py:460
  100.8 0.0 copy-done.4
  100.8 0.9 slice_convert_fusion
  101.7 0.2 slice_add_fusion
  101.9 0.1 copy.41
  102.0 0.2 select_reduce_fusion
  102.3 0.3 copy.43
  102.6 0.3 copy.42
  102.8 1.0 subtract_convert_fusion
  103.8 70.7 %give_back.1 = bf16[128,2048]{1,0:T(8,128)(2,1)} custom-call(bf16[4,2,320,256]{3,2,1,0:T(8,128)(2,1)} %get-tuple-element.7.hid, bf16[256,2048]{1,0:T(8,128)(2,1)} %bitcast.23, bf16[4,128,320]{2,1,0:T(8,128)(2,1)} %get-tuple-element.10.share_hi, bf16[4,128,320]{2,1,0:T(8,128)(2,1)} %get-tuple-element.9.share_lo, bf16[128,2048]{1,0:T(8,128)(2,1)} %copy-done.4), custom_call_target="tpu_custom_call" | custom-call | tf_op jit(solution)/shard_map/give_back/pallas_call | solution.py:494
  174.5 1.9 %copy.52 = bf16[128,2048]{1,0:T(8,128)(2,1)} copy(bf16[128,2048]{1,0:T(8,128)(2,1)} %give_back.1) | data formatting | bytes 1048576
  (9 shorter events, 0.1 us)
Async XLA Ops:
  0.0 24.0 %copy-start.5 = (bf16[128,2048]{1,0:T(8,128)(2,1)S(1)}, bf16[128,2048]{1,0:T(8,128)(2,1)}, u32[]{:S(2)}) copy-start(bf16[128,2048]{1,0:T(8,128)(2,1)} %param.16) | copy-start | bytes 1572868
  2.9 1.0 copy-start
  3.9 0.9 copy-start.1
  4.9 0.9 copy-start.2
  5.8 0.7 copy-start.3
  24.0 4.8 %copy-start.6 = (f32[2048]{0:T(1024)S(1)}, f32[2048]{0:T(1024)}, u32[]{:S(2)}) copy-start(f32[2048]{0:T(1024)} %param.18) | copy-start | bytes 24580
  28.8 71.9 %copy-start.4 = (bf16[128,2048]{1,0:T(8,128)(2,1)}, bf16[128,2048]{1,0:T(8,128)(2,1)S(1)}, u32[]{:S(2)}) copy-start(bf16[128,2048]{1,0:T(8,128)(2,1)S(1)} %get-tuple-element.15.stream) | copy-start | bytes 1572868
